TPU v7x, 32 devices: a whole 2x2x4 slice. The times are simulated.
32 devices in a mesh: grp: 2 (over y), fs: 4 (over z), tp: 4 (over x, core).
Axes of the slice: x: 2, y: 2, z: 4, core: 2. Of those that a mesh axis runs over, the one named last changes fastest.
Arguments:
- stream: bfloat16 [2048, 3072], P('tp', ('grp', 'fs')), parts along dimension 1, may hold values from -6 to 6
- first_gain: float32 [2048], replicated, may hold values from 0.1 to 1.9
- first_gate: float32 [2048, 5632], P('fs', 'tp'), may hold values from -0.125 to 0.125
- first_gate_scale: float32 [5632], P('tp'), may hold values from 0.5 to 2
- first_up: float32 [2048, 5632], P('fs', 'tp'), may hold values from -0.125 to 0.125
- first_up_scale: float32 [5632], P('tp'), may hold values from 0.5 to 2
- first_down: float32 [5632, 2048], P('tp', 'fs'), may hold values from -0.078125 to 0.078125
- first_down_scale: float32 [2048], P('fs'), may hold values from 0.5 to 2
- mixer_gain: float32 [2048], replicated, may hold values from 0.1 to 1.9
- mixer_left: float32 [2048, 1024], P('fs', 'tp'), may hold values from -0.125 to 0.125
- mixer_left_scale: float32 [1024], P('tp'), may hold values from 0.5 to 2
- mixer_right: float32 [2048, 1024], P('fs', 'tp'), may hold values from -0.125 to 0.125
- mixer_right_scale: float32 [1024], P('tp'), may hold values from 0.5 to 2
- channel_gain: float32 [1024], P('tp'), may hold values from 0.1 to 1.9
- spatial: bfloat16 [8, 128, 128], P('tp'), may hold values from -0.5 to 0.5
- spatial_bias: float32 [8, 128], P('tp'), may hold values from 0.1 to 1.9
- mixer_out: float32 [1024, 2048], P('tp', 'fs'), may hold values from -0.1875 to 0.1875
- mixer_out_scale: float32 [2048], P('fs'), may hold values from 0.5 to 2
- second_gain: float32 [2048], replicated, may hold values from 0.1 to 1.9
- second_gate: float32 [2048, 5632], P('fs', 'tp'), may hold values from -0.125 to 0.125
- second_gate_scale: float32 [5632], P('tp'), may hold values from 0.5 to 2
- second_up: float32 [2048, 5632], P('fs', 'tp'), may hold values from -0.125 to 0.125
- second_up_scale: float32 [5632], P('tp'), may hold values from 0.5 to 2
- second_down: float32 [5632, 2048], P('tp', 'fs'), may hold values from -0.078125 to 0.078125
- second_down_scale: float32 [2048], P('fs'), may hold values from 0.5 to 2
Outputs:
- result: bfloat16 [2048, 3072], P('tp', ('grp', 'fs')), parts along dimension 1
There are 2 independent parts, one for each index of `grp`. A program takes and returns all parts, laid end to end along the dimension named above; an argument that names none is the same for every part. Nothing has to cross between parts.
All inputs are finite; a program needn't handle non-finite values.
Results may differ from a plain program's by a relative error of at most 0.02.
Values may be sent and summed in bfloat16 or wider, within the bound.
A program may use at most 128 MiB of HBM per device.

v0:
```python
import jax
import jax.numpy as jnp
from jax import lax
from jax.sharding import PartitionSpec as P

BRANCH = 1024


EPS = 1e-06


def contract(left_side, right_side):
    return lax.dot_general(
        left_side, right_side, (((0,), (0,)), ((), ())), preferred_element_type=jnp.float32
    )


def normed(stream, gain):
    whole_rows = lax.all_gather(stream, "tp", axis=0, tiled=True)
    values = whole_rows.astype(jnp.float32)
    inverse = lax.rsqrt(jnp.mean(values * values, axis=0) + EPS)
    return (values * inverse * gain[:, None]).astype(jnp.bfloat16)


def residual(stream, total, factor):
    return (stream.astype(jnp.float32) + factor * total).astype(jnp.bfloat16)


def swish_hidden(gate, gate_scale, upward, up_scale):
    return (jax.nn.silu(gate * gate_scale[:, None]) * (upward * up_scale[:, None])).astype(
        jnp.bfloat16
    )


def gating_unit(left_pre, right_pre, channel_gain, spatial, spatial_bias):
    left = jax.nn.gelu(left_pre)
    right = jax.nn.gelu(right_pre)
    totals, squares = lax.psum((jnp.sum(right, axis=0), jnp.sum(right * right, axis=0)), "tp")
    average = totals / BRANCH
    inverse = lax.rsqrt(squares / BRANCH - average * average + EPS)
    centred = ((right - average) * inverse * channel_gain[:, None]).astype(jnp.bfloat16)
    local_groups, span = (spatial.shape[0], spatial.shape[1])
    tokens = centred.shape[1]
    blocks = centred.reshape(local_groups, centred.shape[0] // local_groups, tokens // span, span)
    target = lax.broadcasted_iota(jnp.int32, (span, span), 0)
    source = lax.broadcasted_iota(jnp.int32, (span, span), 1)
    masked = jnp.where((source <= target)[None], spatial, jnp.zeros_like(spatial))
    token_mix = jnp.einsum("gts,gcns->gcnt", masked, blocks, preferred_element_type=jnp.float32)
    token_mix = token_mix + spatial_bias[:, None, None, :]
    return (left * token_mix.reshape(centred.shape[0], tokens)).astype(jnp.bfloat16)


def reduce_parts(weight_part, scale_full, hidden, from_mixer):

    def project_cols(piece):
        return contract(piece, hidden) * scale_full[:, None]

    if from_mixer:
        terms = project_cols(lax.all_gather(weight_part, "fs", axis=1, tiled=True))
    else:
        terms = project_cols(lax.all_gather(weight_part, "fs", axis=1, tiled=True))
    return lax.psum_scatter(
        terms.astype(jnp.bfloat16), "tp", scatter_dimension=0, tiled=True
    ).astype(jnp.float32)


def fold_pair(first_part, second_part, normed_rows, from_mixer):

    def add_pair(pieces):
        return (contract(pieces[0], normed_rows), contract(pieces[1], normed_rows))

    if from_mixer:
        return add_pair(
            (
                lax.all_gather(first_part, "fs", axis=0, tiled=True),
                lax.all_gather(second_part, "fs", axis=0, tiled=True),
            )
        )
    return add_pair(
        (
            lax.all_gather(first_part, "fs", axis=0, tiled=True),
            lax.all_gather(second_part, "fs", axis=0, tiled=True),
        )
    )


def local(
    stream,
    first_gain,
    first_gate,
    first_gate_scale,
    first_up,
    first_up_scale,
    first_down,
    first_down_scale,
    mixer_gain,
    mixer_left,
    mixer_left_scale,
    mixer_right,
    mixer_right_scale,
    channel_gain,
    spatial,
    spatial_bias,
    mixer_out,
    mixer_out_scale,
    second_gain,
    second_gate,
    second_gate_scale,
    second_up,
    second_up_scale,
    second_down,
    second_down_scale,
):
    first_cols, mixer_cols, second_cols = (
        lax.all_gather(first_down_scale, "fs", axis=0, tiled=True),
        lax.all_gather(mixer_out_scale, "fs", axis=0, tiled=True),
        lax.all_gather(second_down_scale, "fs", axis=0, tiled=True),
    )
    bf = jnp.bfloat16
    first_rows = normed(stream, first_gain)
    gate, upward = fold_pair(first_gate.astype(bf), first_up.astype(bf), first_rows, False)
    hidden = swish_hidden(gate, first_gate_scale, upward, first_up_scale)
    stream = residual(stream, reduce_parts(first_down.astype(bf), first_cols, hidden, False), 0.5)
    mixer_rows = normed(stream, mixer_gain)
    left_pre, right_pre = fold_pair(mixer_left.astype(bf), mixer_right.astype(bf), mixer_rows, True)
    gated = gating_unit(
        left_pre * mixer_left_scale[:, None],
        right_pre * mixer_right_scale[:, None],
        channel_gain,
        spatial,
        spatial_bias,
    )
    stream = residual(stream, reduce_parts(mixer_out.astype(bf), mixer_cols, gated, True), 1.0)
    second_rows = normed(stream, second_gain)
    gate, upward = fold_pair(second_gate.astype(bf), second_up.astype(bf), second_rows, False)
    hidden = swish_hidden(gate, second_gate_scale, upward, second_up_scale)
    stream = residual(stream, reduce_parts(second_down.astype(bf), second_cols, hidden, False), 0.5)
    return stream


def solution(mesh):
    return jax.shard_map(
        local,
        mesh=mesh,
        in_specs=(
            P("tp", ("grp", "fs")),
            P(),
            P("fs", "tp"),
            P("tp"),
            P("fs", "tp"),
            P("tp"),
            P("tp", "fs"),
            P("fs"),
            P(),
            P("fs", "tp"),
            P("tp"),
            P("fs", "tp"),
            P("tp"),
            P("tp"),
            P("tp", None, None),
            P("tp", None),
            P("tp", "fs"),
            P("fs"),
            P(),
            P("fs", "tp"),
            P("tp"),
            P("fs", "tp"),
            P("tp"),
            P("tp", "fs"),
            P("fs"),
        ),
        out_specs=P("tp", ("grp", "fs")),
        check_vma=False,
    )
```

profile of v0, /device:TPU:0, one launch (start us, length us, event | category | flops | bytes accessed | tf_op | source)
XLA Modules:
  0.0 921.2 jit_solution(8410099119789892153)
XLA Ops:
  7.3 3.2 convert_element_type.105
  15.2 13.6 %all-gather = f32[4,1,512]{2,1,0:T(1,128)S(1)} all-gather(f32[1,1,512]{2,1,0:T(1,128)S(1)} %bitcast.75), channel_id=1, replica_groups=mesh['grp'=2,'fs'=4,'tp'=4] {'fs'}, dimensions={0}, use_global_device_ids=true | all-gather | bytes 10240 | tf_op jit(solution)/shard_map/all_gather | solution.py:115
  33.1 106.4 %all-gather.18.cloned.1.call-done = bf16[2048,1408]{1,0:T(8,128)(2,1)} async-done(((bf16[512,1408]{1,0:T(8,128)(2,1)}), bf16[2048,1408]{1,0:T(8,128)(2,1)}) %all-gather.18.cloned.1.call-update) | async-done | bytes 5767184 | tf_op jit(solution)/shard_map/all_gather | solution.py:81
  139.6 7.2 fusion.9
  146.8 99.4 %all-gather.20.cloned.1.call-done = bf16[2048,1408]{1,0:T(8,128)(2,1)} async-done(((bf16[512,1408]{1,0:T(8,128)(2,1)}), bf16[2048,1408]{1,0:T(8,128)(2,1)}) %all-gather.20.cloned.1.call-update) | async-done | bytes 5767184 | tf_op jit(solution)/shard_map/all_gather | solution.py:82
  246.1 106.4 %all-gather.22.cloned.1.call-done = bf16[1408,2048]{1,0:T(8,128)(2,1)} async-done(((bf16[1408,512]{1,0:T(8,128)(2,1)}), bf16[1408,2048]{1,0:T(8,128)(2,1)}) %all-gather.22.cloned.1.call-update) | async-done | bytes 5767184 | tf_op jit(solution)/shard_map/all_gather | solution.py:61
  352.5 11.7 %fusion.17 = bf16[2048,384]{0,1:T(8,128)(2,1)} fusion(bf16[1408,2048]{1,0:T(8,128)(2,1)} %all-gather.22.cloned.1.call-done, f32[2048]{0:T(1024)S(1)} %bitcast.73, bf16[2048,1408]{1,0:T(8,128)(2,1)} %all-gather.20.cloned.1.call-done, f32[1408,384]{0,1:T(8,128)} %fusion.9, f32[1408]{0:T(1024)S(1)} %copy-done.20, bf16[2048,384]{1,0:T(8,128)(2,1)S(1)} %copy-done.6, ...), kind=kOutput, calls=%fused_computation.30 | convolution fusion | flops 4437688320 | bytes 16866304 | tf_op jit(solution)/shard_map/dot_general | solution.py:13
  364.5 26.1 %reduce-scatter.4.cloned.1.call-done = bf16[512,384]{0,1:T(8,128)(2,1)} async-done(((bf16[2048,384]{0,1:T(8,128)(2,1)}), bf16[512,384]{0,1:T(8,128)(2,1)}) %reduce-scatter.4.cloned.1.call-update) | async-done | bytes 393232 | tf_op jit(solution)/shard_map/reduce_scatter | solution.py:62
  395.1 12.0 %all-gather.1 = f32[4,1,512]{2,1,0:T(1,128)S(1)} all-gather(f32[1,1,512]{2,1,0:T(1,128)S(1)} %bitcast.76), channel_id=1, replica_groups=mesh['grp'=2,'fs'=4,'tp'=4] {'fs'}, dimensions={0}, use_global_device_ids=true | all-gather | bytes 10240 | tf_op jit(solution)/shard_map/all_gather | solution.py:116
  407.1 5.2 all-gather.24.cloned.1.call-done
  414.2 27.8 %all-gather.28.cloned.1.call-done = bf16[2048,256]{1,0:T(8,128)(2,1)} async-done(((bf16[512,256]{1,0:T(8,128)(2,1)}), bf16[2048,256]{1,0:T(8,128)(2,1)}) %all-gather.28.cloned.1.call-update) | async-done | bytes 1048592 | tf_op jit(solution)/shard_map/all_gather | solution.py:76
  444.4 6.2 all-reduce
  451.4 19.4 %all-gather.26.cloned.1.call-done = bf16[2048,256]{1,0:T(8,128)(2,1)} async-done(((bf16[512,256]{1,0:T(8,128)(2,1)}), bf16[2048,256]{1,0:T(8,128)(2,1)}) %all-gather.26.cloned.1.call-update) | async-done | bytes 1048592 | tf_op jit(solution)/shard_map/all_gather | solution.py:75
  470.9 29.0 %all-gather.30.cloned.1.call-done = bf16[256,2048]{1,0:T(8,128)(2,1)} async-done(((bf16[256,512]{1,0:T(8,128)(2,1)}), bf16[256,2048]{1,0:T(8,128)(2,1)}) %all-gather.30.cloned.1.call-update) | async-done | bytes 1048592 | tf_op jit(solution)/shard_map/all_gather | solution.py:59
  499.8 4.7 fusion.18
  504.6 27.5 %reduce-scatter.6.cloned.1.call-done = bf16[512,384]{0,1:T(8,128)(2,1)} async-done(((bf16[2048,384]{0,1:T(8,128)(2,1)}), bf16[512,384]{0,1:T(8,128)(2,1)}) %reduce-scatter.6.cloned.1.call-update) | async-done | bytes 393232 | tf_op jit(solution)/shard_map/reduce_scatter | solution.py:62
  535.5 3.2 convert_element_type.129
  540.2 12.0 %all-gather.2 = f32[4,1,512]{2,1,0:T(1,128)S(1)} all-gather(f32[1,1,512]{2,1,0:T(1,128)S(1)} %bitcast.77), channel_id=1, replica_groups=mesh['grp'=2,'fs'=4,'tp'=4] {'fs'}, dimensions={0}, use_global_device_ids=true | all-gather | bytes 10240 | tf_op jit(solution)/shard_map/all_gather | solution.py:117
  555.5 106.3 %all-gather.34.cloned.1.call-done = bf16[2048,1408]{1,0:T(8,128)(2,1)} async-done(((bf16[512,1408]{1,0:T(8,128)(2,1)}), bf16[2048,1408]{1,0:T(8,128)(2,1)}) %all-gather.34.cloned.1.call-update) | async-done | bytes 5767184 | tf_op jit(solution)/shard_map/all_gather | solution.py:81
  661.9 7.1 fusion.12
  669.0 99.4 %all-gather.36.cloned.1.call-done = bf16[2048,1408]{1,0:T(8,128)(2,1)} async-done(((bf16[512,1408]{1,0:T(8,128)(2,1)}), bf16[2048,1408]{1,0:T(8,128)(2,1)}) %all-gather.36.cloned.1.call-update) | async-done | bytes 5767184 | tf_op jit(solution)/shard_map/all_gather | solution.py:82
  768.4 106.4 %all-gather.38.cloned.1.call-done = bf16[1408,2048]{1,0:T(8,128)(2,1)} async-done(((bf16[1408,512]{1,0:T(8,128)(2,1)}), bf16[1408,2048]{1,0:T(8,128)(2,1)}) %all-gather.38.cloned.1.call-update) | async-done | bytes 5767184 | tf_op jit(solution)/shard_map/all_gather | solution.py:61
  874.8 11.4 %fusion.19 = bf16[2048,384]{0,1:T(8,128)(2,1)} fusion(bf16[1408,2048]{1,0:T(8,128)(2,1)} %all-gather.38.cloned.1.call-done, f32[2048]{0:T(1024)S(1)} %bitcast.74, bf16[2048,1408]{1,0:T(8,128)(2,1)} %all-gather.36.cloned.1.call-done, f32[1408,384]{0,1:T(8,128)} %fusion.12, f32[1408]{0:T(1024)S(1)} %copy-done.24, bf16[2048,384]{0,1:T(8,128)(2,1)S(1)} %copy-done.7, ...), kind=kOutput, calls=%fused_computation.32 | convolution fusion | flops 4437688320 | bytes 16866304 | tf_op jit(solution)/shard_map/dot_general | solution.py:13
  886.2 26.4 %reduce-scatter.8.cloned.1.call-done = bf16[512,384]{0,1:T(8,128)(2,1)} async-done(((bf16[2048,384]{0,1:T(8,128)(2,1)}), bf16[512,384]{0,1:T(8,128)(2,1)}) %reduce-scatter.8.cloned.1.call-update) | async-done | bytes 393232 | tf_op jit(solution)/shard_map/reduce_scatter | solution.py:62
  (111 shorter events, 29.5 us)
Async XLA Ops:
  6.5 24.7 %all-gather.16.cloned.1.call-start = ((), (), s32[]{:S(2)}) async-start(), calls=%async_computation.3 | async-start | bytes 1966080 | tf_op jit(solution)/shard_map/all_gather | solution.py:19
  7.3 132.3 %all-gather.18.cloned.1.call-start = ((), (), s32[]{:S(2)}) async-start(), calls=%async_computation.4 | async-start | bytes 7208960 | tf_op jit(solution)/shard_map/all_gather | solution.py:81
  10.6 235.5 %all-gather.20.cloned.1.call-start = ((), (), s32[]{:S(2)}) async-start(), calls=%async_computation.5 | async-start | bytes 7208960 | tf_op jit(solution)/shard_map/all_gather | solution.py:82
  12.0 340.6 %all-gather.22.cloned.1.call-start = ((), (), s32[]{:S(2)}) async-start(), calls=%async_computation.6 | async-start | bytes 7208960 | tf_op jit(solution)/shard_map/all_gather | solution.py:61
  15.1 124.5 %copy-start.18 = (f32[1408]{0:T(1024)S(1)}, f32[1408]{0:T(1024)}, u32[]{:S(2)}) copy-start(f32[1408]{0:T(1024)} %param.28) | copy-start | bytes 16900
  15.1 124.5 %copy-start.19 = (f32[2048]{0:T(1024)S(1)}, f32[2048]{0:T(1024)}, u32[]{:S(2)}) copy-start(f32[2048]{0:T(1024)} %param.26) | copy-start | bytes 24580
  15.1 375.5 %reduce-scatter.4.cloned.1.call-start = ((), (), s32[]{:S(2)}) async-start(), calls=%async_computation.7 | async-start | bytes 1966080 | tf_op jit(solution)/shard_map/reduce_scatter | solution.py:62
  33.1 319.4 %copy-start.6 = (bf16[2048,384]{1,0:T(8,128)(2,1)S(1)}, bf16[2048,384]{1,0:T(8,128)(2,1)}, u32[]{:S(2)}) copy-start(bf16[2048,384]{1,0:T(8,128)(2,1)} %all-gather.16.cloned.1.call-done) | copy-start | bytes 4718596
  33.1 319.4 %copy-start.20 = (f32[1408]{0:T(1024)S(1)}, f32[1408]{0:T(1024)}, u32[]{:S(2)}) copy-start(f32[1408]{0:T(1024)} %param.30) | copy-start | bytes 16900
  364.3 48.1 %all-gather.24.cloned.1.call-start = ((), (), s32[]{:S(2)}) async-start(), calls=%async_computation.8 | async-start | bytes 1966080 | tf_op jit(solution)/shard_map/all_gather | solution.py:19
  392.5 49.4 %all-gather.28.cloned.1.call-start = ((), (), s32[]{:S(2)}) async-start(), calls=%async_computation.10 | async-start | bytes 1310720 | tf_op jit(solution)/shard_map/all_gather | solution.py:76
  393.4 77.5 %all-gather.26.cloned.1.call-start = ((), (), s32[]{:S(2)}) async-start(), calls=%async_computation.9 | async-start | bytes 1310720 | tf_op jit(solution)/shard_map/all_gather | solution.py:75
  394.2 105.6 %all-gather.30.cloned.1.call-start = ((), (), s32[]{:S(2)}) async-start(), calls=%async_computation.11 | async-start | bytes 1310720 | tf_op jit(solution)/shard_map/all_gather | solution.py:59
  395.0 137.0 %reduce-scatter.6.cloned.1.call-start = ((), (), s32[]{:S(2)}) async-start(), calls=%async_computation.12 | async-start | bytes 1966080 | tf_op jit(solution)/shard_map/reduce_scatter | solution.py:62
  444.4 55.4 %copy-start.5 = (bf16[2048,384]{0,1:T(8,128)(2,1)S(1)}, bf16[2048,384]{0,1:T(8,128)(2,1)}, u32[]{:S(2)}) copy-start(bf16[2048,384]{0,1:T(8,128)(2,1)} %all-gather.24.cloned.1.call-done) | copy-start | bytes 4718596
  504.5 49.2 %all-gather.32.cloned.1.call-start = ((), (), s32[]{:S(2)}) async-start(), calls=%async_computation.13 | async-start | bytes 1966080 | tf_op jit(solution)/shard_map/all_gather | solution.py:19
  533.9 127.9 %all-gather.34.cloned.1.call-start = ((), (), s32[]{:S(2)}) async-start(), calls=%async_computation.14 | async-start | bytes 7208960 | tf_op jit(solution)/shard_map/all_gather | solution.py:81
  535.5 232.9 %all-gather.36.cloned.1.call-start = ((), (), s32[]{:S(2)}) async-start(), calls=%async_computation.15 | async-start | bytes 7208960 | tf_op jit(solution)/shard_map/all_gather | solution.py:82
  538.8 336.0 %all-gather.38.cloned.1.call-start = ((), (), s32[]{:S(2)}) async-start(), calls=%async_computation.16 | async-start | bytes 7208960 | tf_op jit(solution)/shard_map/all_gather | solution.py:61
  540.1 121.7 %copy-start.22 = (f32[1408]{0:T(1024)S(1)}, f32[1408]{0:T(1024)}, u32[]{:S(2)}) copy-start(f32[1408]{0:T(1024)} %param.45) | copy-start | bytes 16900
  540.2 121.7 %copy-start.23 = (f32[2048]{0:T(1024)S(1)}, f32[2048]{0:T(1024)}, u32[]{:S(2)}) copy-start(f32[2048]{0:T(1024)} %param.43) | copy-start | bytes 24580
  540.2 372.5 %reduce-scatter.8.cloned.1.call-start = ((), (), s32[]{:S(2)}) async-start(), calls=%async_computation.17 | async-start | bytes 1966080 | tf_op jit(solution)/shard_map/reduce_scatter | solution.py:62
  555.5 319.3 %copy-start.7 = (bf16[2048,384]{0,1:T(8,128)(2,1)S(1)}, bf16[2048,384]{0,1:T(8,128)(2,1)}, u32[]{:S(2)}) copy-start(bf16[2048,384]{0,1:T(8,128)(2,1)} %all-gather.32.cloned.1.call-done) | copy-start | bytes 4718596
  555.5 319.3 %copy-start.24 = (f32[1408]{0:T(1024)S(1)}, f32[1408]{0:T(1024)}, u32[]{:S(2)}) copy-start(f32[1408]{0:T(1024)} %param.47) | copy-start | bytes 16900
  (18 other events, 503.7 us)
Sparse Core Ops, SparseCore 0:
  8.9 22.3 all-gather.15
  32.8 106.6 all-gather.17
  141.1 104.9 all-gather.19
  247.5 104.9 all-gather.21
  364.4 26.2 reduce-scatter.3
  392.6 19.6 all-gather.23
  413.9 27.9 all-gather.27
  443.5 27.3 all-gather.25
  472.4 27.3 all-gather.29
  504.7 27.3 reduce-scatter.5
  534.0 19.6 all-gather.31
  555.2 106.6 all-gather.33
  663.4 104.9 all-gather.35
  769.8 104.9 all-gather.37
  886.3 26.2 reduce-scatter.7
where the time goes:
time: 922 us; the launch traced here: 921 us
  waiting for transfers between devices  791 us (86%)
  matrix products  44.8 us (5%)
  blocking collectives  43.8 us (5%)
  other arithmetic  26.1 us (3%)
  between operations  13.6 us (1%)
    all_gather x3, waiting for transfers between devices, reduce_parts(): terms = project_cols(lax.all_gather(weight_part, 'fs', axis=1, tiled=True))  242 us
    all_gather x3, waiting for transfers between devices, fold_pair(): lax.all_gather(first_part, 'fs', axis=0, tiled=True)  232 us
    all_gather x3, waiting for transfers between devices, fold_pair(): lax.all_gather(second_part, 'fs', axis=0, tiled=True)  227 us
    reduce_scatter x3, waiting for transfers between devices, reduce_parts(): lax.psum_scatter(terms.astype(jnp.bfloat16), 'tp', scatter_dimension=0, t...  80 us
    dot_general x6, matrix products, contract(): lax.dot_general(left_side, right_side, (((0,), (0,)), ((), ())), preferre...  44.5 us
  transfers between devices with their start and end apart: 15, of which 15 were waited for; matrix products, arithmetic and copies ran while one was open for 4% of the time, Pallas kernels for 0%

commit v1 on v0

v1 whole, which is shorter than its diff:
```python
import jax
import jax.numpy as jnp
from jax import lax
from jax.sharding import PartitionSpec as P


BRANCH = 1024


EPS = 1e-06
LAST_PARTS = 2


def contract(left_side, right_side):
    return lax.dot_general(
        left_side, right_side, (((0,), (0,)), ((), ())), preferred_element_type=jnp.float32
    )


CORES = 2


def shifted(block, axis_name, step):
    count = lax.axis_size(axis_name)
    return lax.ppermute(block, axis_name, [(at, (at + step) % count) for at in range(count)])


def to_same_core(block, step):
    count = lax.axis_size("tp")
    return lax.ppermute(
        block, "tp", [(at, (at + step * CORES) % count) for at in range(count)]
    )


def to_other_core(block):
    return lax.ppermute(block, "tp", [(at, at ^ 1) for at in range(lax.axis_size("tp"))])


def pick(blocks, index):
    count = len(blocks)
    if count == 1:
        return blocks[0]
    index = lax.rem(index + count, count)
    found = blocks[0]
    for at in range(1, count):
        found = jnp.where(index == at, blocks[at], found)
    return found


def chip_and_core():
    place = lax.axis_index("tp")
    return lax.div(place, CORES), lax.rem(place, CORES)


def gather_rows(block):
    chips = lax.axis_size("tp") // CORES
    chip, core = chip_and_core()
    held = jnp.stack([block] + [to_same_core(block, step) for step in range(1, chips)])
    other = to_other_core(held)
    found = []
    for at_chip in range(chips):
        mine = pick([held[step] for step in range(chips)], chip - at_chip)
        theirs = pick([other[step] for step in range(chips)], chip - at_chip)
        found += [jnp.where(core == 0, mine, theirs), jnp.where(core == 0, theirs, mine)]
    return jnp.concatenate(found)


def scatter_sum(terms):
    chips = lax.axis_size("tp") // CORES
    chip, core = chip_and_core()
    blocks = terms.reshape((chips, CORES, -1) + terms.shape[1:])
    mine = jnp.where(core == 0, blocks[:, 0], blocks[:, 1])
    passed = jnp.where(core == 0, blocks[:, 1], blocks[:, 0])
    pairs = mine.astype(jnp.float32) + to_other_core(passed).astype(jnp.float32)
    total = pick([pairs[at] for at in range(chips)], chip)
    for step in range(1, chips):
        sent = pick([pairs[at] for at in range(chips)], chip + step).astype(jnp.bfloat16)
        total = total + to_same_core(sent, step).astype(jnp.float32)
    return total


def share_of(weight_part, axis, back):
    shares = lax.axis_size("grp")
    width = weight_part.shape[axis] // shares
    index = lax.rem(lax.axis_index("grp") - back + shares, shares)
    return lax.dynamic_slice_in_dim(weight_part, index * width, width, axis).astype(jnp.bfloat16)


def ring_place(step):
    return lax.rem(lax.axis_index("fs") + step, lax.axis_size("fs"))


def exchange(share, following):
    blocks = lax.all_gather(share, "fs", axis=0, tiled=False)
    rest = jnp.stack(
        [
            lax.dynamic_index_in_dim(blocks, ring_place(step), 0, keepdims=False)
            for step in range(1, lax.axis_size("fs"))
        ]
    )
    if following is not None:
        rest, following = lax.optimization_barrier((rest, following))
    rests = [shifted(rest, "grp", back) for back in range(1, lax.axis_size("grp"))]
    return blocks, rests, following


def flat(blocks):
    return blocks.reshape((-1,) + blocks.shape[2:])


def joined(blocks, rests, locals_of):
    pieces = [flat(blocks)]
    for rest, own in zip(rests, locals_of):
        pieces += [own, flat(rest)]
    return jnp.concatenate(pieces)


def rows_in_order(normed_rows):
    shares, count = (lax.axis_size("grp"), lax.axis_size("fs"))
    rows = normed_rows.reshape(count, shares, -1, normed_rows.shape[1])

    def at(place, back):
        index = lax.rem(lax.axis_index("grp") - back + shares, shares)
        return lax.dynamic_slice(
            rows, (place, index, 0, 0), (1, 1, rows.shape[2], rows.shape[3])
        ).reshape(rows.shape[2:])

    pieces = [at(place, 0) for place in range(count)]
    for back in range(1, shares):
        pieces += [at(ring_place(step), back) for step in range(count)]
    return jnp.concatenate(pieces)


def column_terms(blocks, rests, locals_of, scale, hidden, transposed):
    shares, count = (lax.axis_size("grp"), lax.axis_size("fs"))
    place = lax.axis_index("fs")

    def product(pieces):
        form = "bnk,kt->bnt" if transposed else "bkn,kt->bnt"
        return jnp.einsum(form, pieces, hidden, preferred_element_type=jnp.float32)

    def scale_at(back):
        index = lax.rem(lax.axis_index("grp") - back + shares, shares)
        return lax.dynamic_index_in_dim(scale, index, 1, keepdims=False)[:, :, None]

    own = (product(blocks) * scale_at(0)).astype(jnp.bfloat16)
    found = [[own[at] for at in range(count)]]
    for back in range(1, shares):
        turned = scale_at(back)
        here = lax.dynamic_index_in_dim(turned, place, 0)
        local = (product(locals_of[back - 1][None]) * here).astype(jnp.bfloat16)
        away = jnp.stack(
            [
                lax.dynamic_index_in_dim(turned, ring_place(step), 0, keepdims=False)
                for step in range(1, count)
            ]
        )
        rest = (product(rests[back - 1]) * away).astype(jnp.bfloat16)
        ring = [local[0]] + [rest[at] for at in range(count - 1)]
        found.append([pick(ring, at - place) for at in range(count)])
    grp = lax.axis_index("grp")
    return [
        [pick([found[back][at] for back in range(shares)], grp - share) for share in range(shares)]
        for at in range(count)
    ]


def normed(stream, gain):
    whole_rows = gather_rows(stream)
    values = whole_rows.astype(jnp.float32)
    inverse = lax.rsqrt(jnp.mean(values * values, axis=0) + EPS)
    return (values * inverse * gain[:, None]).astype(jnp.bfloat16)


def residual(stream, total, factor):
    return (stream.astype(jnp.float32) + factor * total).astype(jnp.bfloat16)


def swish_hidden(gate, gate_scale, upward, up_scale):
    return (jax.nn.silu(gate * gate_scale[:, None]) * (upward * up_scale[:, None])).astype(
        jnp.bfloat16
    )


def gating_unit(left_pre, right_pre, channel_gain, spatial, spatial_bias):
    left = jax.nn.gelu(left_pre)
    right = jax.nn.gelu(right_pre)
    totals, squares = lax.psum((jnp.sum(right, axis=0), jnp.sum(right * right, axis=0)), "tp")
    average = totals / BRANCH
    inverse = lax.rsqrt(squares / BRANCH - average * average + EPS)
    centred = ((right - average) * inverse * channel_gain[:, None]).astype(jnp.bfloat16)
    local_groups, span = (spatial.shape[0], spatial.shape[1])
    tokens = centred.shape[1]
    blocks = centred.reshape(local_groups, centred.shape[0] // local_groups, tokens // span, span)
    target = lax.broadcasted_iota(jnp.int32, (span, span), 0)
    source = lax.broadcasted_iota(jnp.int32, (span, span), 1)
    masked = jnp.where((source <= target)[None], spatial, jnp.zeros_like(spatial))
    token_mix = jnp.einsum("gts,gcns->gcnt", masked, blocks, preferred_element_type=jnp.float32)
    token_mix = token_mix + spatial_bias[:, None, None, :]
    return (left * token_mix.reshape(centred.shape[0], tokens)).astype(jnp.bfloat16)


def layer(
    stream,
    first_gain,
    first_gate,
    first_gate_scale,
    first_up,
    first_up_scale,
    first_down,
    first_down_scale,
    mixer_gain,
    mixer_left,
    mixer_left_scale,
    mixer_right,
    mixer_right_scale,
    channel_gain,
    spatial,
    spatial_bias,
    mixer_out,
    mixer_out_scale,
    second_gain,
    second_gate,
    second_gate_scale,
    second_up,
    second_up_scale,
    second_down,
    second_down_scale,
):
    shares, count = (lax.axis_size("grp"), lax.axis_size("fs"))
    backs = range(1, shares)
    cols = lax.all_gather(
        jnp.stack([first_down_scale, mixer_out_scale, second_down_scale]), "fs", axis=0, tiled=False
    )
    cols = cols.reshape(count, 3, shares, -1)

    def mixer_share(back):
        return jnp.stack(
            [
                share_of(mixer_left, 0, back),
                share_of(mixer_right, 0, back),
                share_of(mixer_out, 1, back).T,
            ]
        )

    def rows_share(weight):
        return lambda back: share_of(weight, 0, back)

    def cols_share(weight, part, parts):
        def cut(back):
            share = share_of(weight, 1, back)
            width = share.shape[1] // parts
            return share[:, part * width : (part + 1) * width]

        return cut

    units = (
        rows_share(first_gate),
        rows_share(first_up),
        cols_share(first_down, 0, 1),
        mixer_share,
        rows_share(second_gate),
        rows_share(second_up),
    ) + tuple(cols_share(second_down, part, LAST_PARTS) for part in range(LAST_PARTS))
    ready = []
    share = units[0](0)
    for number, unit in enumerate(units):
        following = units[number + 1](0) if number + 1 < len(units) else None
        blocks, rests, share = exchange(share, following)
        ready.append((blocks, rests, [unit(back) for back in backs]))

    def half_step(stream, gain, gate_unit, gate_scale, up_unit, up_scale, down_units, down_cols):
        rows = rows_in_order(normed(stream, gain))
        gate = contract(joined(*gate_unit), rows)
        upward = contract(joined(*up_unit), rows)
        hidden = swish_hidden(gate, gate_scale, upward, up_scale)
        width = down_cols.shape[2] // len(down_units)
        terms = [
            column_terms(
                *unit, down_cols[:, :, part * width : (part + 1) * width], hidden, False
            )
            for part, unit in enumerate(down_units)
        ]
        ordered = [
            term[at][share] for at in range(count) for share in range(shares) for term in terms
        ]
        return residual(stream, scatter_sum(jnp.concatenate(ordered)), 0.5)

    stream = half_step(
        stream, first_gain, ready[0], first_gate_scale, ready[1], first_up_scale, ready[2:3], cols[:, 0]
    )
    rows = rows_in_order(normed(stream, mixer_gain))
    blocks, rests, local_shares = ready[3]

    def mixer_unit(index):
        return (
            blocks[:, index],
            [rest[:, index] for rest in rests],
            [local_share[index] for local_share in local_shares],
        )

    left_pre = contract(joined(*mixer_unit(0)), rows)
    right_pre = contract(joined(*mixer_unit(1)), rows)
    gated = gating_unit(
        left_pre * mixer_left_scale[:, None],
        right_pre * mixer_right_scale[:, None],
        channel_gain,
        spatial,
        spatial_bias,
    )
    terms = column_terms(*mixer_unit(2), cols[:, 1], gated, True)
    terms = jnp.concatenate([terms[at][share] for at in range(count) for share in range(shares)])
    stream = residual(stream, scatter_sum(terms), 1.0)
    return half_step(
        stream, second_gain, ready[4], second_gate_scale, ready[5], second_up_scale, ready[6:], cols[:, 2]
    )


def solution(mesh):
    return jax.shard_map(
        layer,
        mesh=mesh,
        in_specs=(
            P("tp", ("grp", "fs")),
            P(),
            P("fs", "tp"),
            P("tp"),
            P("fs", "tp"),
            P("tp"),
            P("tp", "fs"),
            P("fs"),
            P(),
            P("fs", "tp"),
            P("tp"),
            P("fs", "tp"),
            P("tp"),
            P("tp"),
            P("tp", None, None),
            P("tp", None),
            P("tp", "fs"),
            P("fs"),
            P(),
            P("fs", "tp"),
            P("tp"),
            P("fs", "tp"),
            P("tp"),
            P("tp", "fs"),
            P("fs"),
        ),
        out_specs=P("tp", ("grp", "fs")),
        check_vma=False,
    )
```

time: 922 us -> 640 us (0.69)
  waiting for transfers between devices: 791 us -> 430 us
  local copies, waits for them, and re-layouts: 1.49 us -> 63.2 us
  blocking collectives: 43.8 us -> 19.7 us
  starting transfers between devices: 0.77 us -> 18.4 us
  other arithmetic: 26.1 us -> 40.7 us
    all_gather x12 -> x8, waiting for transfers between devices: 710 us -> 224 us  [exchange(): blocks = lax.all_gather(share, 'fs', axis=0, tiled=False)]
    ppermute x0 -> x20, waiting for transfers between devices: none -> 205 us  [the longest x8 157 us: shifted(): lax.ppermute(block, axis_name, [(at, (at + step) % count) for at in range...]
    reduce_scatter x3 -> x0, waiting for transfers between devices: 80 us -> none  [reduce_parts(): lax.psum_scatter(terms.astype(jnp.bfloat16), 'tp', scatter_dimension=0, t...]
    unnamed x55 -> x124, local copies, waits for them, and re-layouts: 0.32 us -> 29.2 us
    all_gather x3 -> x1, blocking collectives: 37.6 us -> 13.6 us  [layer(): lax.all_gather(jnp.stack([first_down_scale, mixer_out_scale, second_down_...]
    another operation x0 -> x14, other arithmetic: none -> 19.4 us  [the longest x8 14.7 us: exchange(): jnp.stack([lax.dynamic_index_in_dim(blocks, ring_place(step), 0, keepdims...]
    dot_general x6, matrix products: 44.5 us -> 25.7 us  [contract(): lax.dot_general(left_side, right_side, (((0,), (0,)), ((), ())), preferre...]
    ppermute x0 -> x20, starting transfers between devices: none -> 17.7 us  [the longest x8 10.2 us: shifted(): lax.ppermute(block, axis_name, [(at, (at + step) % count) for at in range...]
  transfers between devices with their start and end apart: 15 -> 28, of which waited for: 15 -> 22; matrix products, arithmetic and copies ran while one was open for 4% -> 20% of each run, Pallas kernels for 0% -> 0%
where the time goes in v1:
time: 640 us; the launch traced here: 630 us
  waiting for transfers between devices  430 us (67%)
  local copies, waits for them, and re-layouts  63.2 us (10%)
  matrix products  43.4 us (7%)
  other arithmetic  40.7 us (6%)
  blocking collectives  19.7 us (3%)
  starting transfers between devices  18.4 us (3%)
  between operations  14.9 us (2%)
    all_gather x8, waiting for transfers between devices, exchange(): blocks = lax.all_gather(share, 'fs', axis=0, tiled=False)  224 us
    ppermute x8, waiting for transfers between devices, shifted(): lax.ppermute(block, axis_name, [(at, (at + step) % count) for at in range...  157 us
    ppermute x6, waiting for transfers between devices, to_same_core(): lax.ppermute(block, 'tp', [(at, (at + step * CORES) % count) for at in ra...  42.9 us
    unnamed x124, local copies, waits for them, and re-layouts  29.2 us
    dot_general x6, matrix products, contract(): lax.dot_general(left_side, right_side, (((0,), (0,)), ((), ())), preferre...  25.7 us
    dot_general x12, matrix products, product(): return jnp.einsum(form, pieces, hidden, preferred_element_type=jnp.float32)  17.5 us
    convert_element_type x6, local copies, waits for them, and re-layouts, share_of(): lax.dynamic_slice_in_dim(weight_part, index * width, width, axis)  14.7 us
    another operation x8, other arithmetic, exchange(): jnp.stack([lax.dynamic_index_in_dim(blocks, ring_place(step), 0, keepdims...  14.7 us
  transfers between devices with their start and end apart: 28, of which 22 were waited for; matrix products, arithmetic and copies ran while one was open for 20% of the time, Pallas kernels for 0%

profile of v1, /device:TPU:0, one launch (start us, length us, event | category | flops | bytes accessed | tf_op | source)
XLA Modules:
  0.0 630.5 jit_solution(18390546047051894415)
XLA Ops:
  9.9 4.3 dynamic-slice_convert_fusion.2
  14.2 57.6 %all-gather.19.cloned.1.call-done = bf16[1024,1408]{1,0:T(8,128)(2,1)} async-done(((bf16[256,1408]{1,0:T(8,128)(2,1)}), bf16[1024,1408]{1,0:T(8,128)(2,1)}) %all-gather.19.cloned.1.call-update) | async-done | bytes 2883600 | tf_op jit(solution)/shard_map/all_gather | solution.py:94
  76.2 56.9 %all-gather.21.cloned.1.call-done = bf16[1024,1408]{1,0:T(8,128)(2,1)} async-done(((bf16[256,1408]{1,0:T(8,128)(2,1)}), bf16[1024,1408]{1,0:T(8,128)(2,1)}) %all-gather.21.cloned.1.call-update) | async-done | bytes 2883600 | tf_op jit(solution)/shard_map/all_gather | solution.py:94
  139.9 13.6 %all-gather.9 = f32[4,3,512]{2,1,0:T(4,128)S(1)} all-gather(f32[1,3,512]{2,1,0:T(4,128)S(1)} %maximum_bitcast_fusion), channel_id=5, replica_groups=mesh['grp'=2,'fs'=4,'tp'=4] {'fs'}, dimensions={0}, use_global_device_ids=true | all-gather | bytes 30720 | tf_op jit(solution)/shard_map/all_gather | solution.py:232
  170.8 23.9 %all-gather.23.cloned.1.call-done = bf16[5632,256]{1,0:T(8,128)(2,1)} async-done(((bf16[1408,256]{1,0:T(8,128)(2,1)}), bf16[5632,256]{1,0:T(8,128)(2,1)}) %all-gather.23.cloned.1.call-update) | async-done | bytes 2883600 | tf_op jit(solution)/shard_map/all_gather | solution.py:94
  212.8 5.4 fusion.33
  218.3 40.9 %collective-permute-done.4 = bf16[3,256,1408]{2,1,0:T(8,128)(2,1)} collective-permute-done((bf16[3,256,1408]{2,1,0:T(8,128)(2,1)}, bf16[3,256,1408]{2,1,0:T(8,128)(2,1)}, u32[]{:S(2)}, u32[]{:S(2)}) %collective-permute-start.4) | collective-permute-done | bytes 2162720 | tf_op jit(solution)/shard_map/ppermute | solution.py:25
  259.1 6.6 %multiply_convert_fusion.4 = bf16[1408,384]{1,0:T(8,128)(2,1)} fusion(f32[1408,384]{1,0:T(8,128)S(1)} %fusion.33, f32[1408]{0:T(1024)S(1)} %copy-done.37, bf16[2048,384]{1,0:T(8,128)(2,1)} %bitcast_dynamic-update-slice_fusion.16, bf16[768,1408]{1,0:T(8,128)(2,1)} %bitcast.21, bf16[256,1408]{1,0:T(8,128)(2,1)S(1)} %copy-done.16, ...), kind=kOutput, calls=%fused_computation.40 | convolution fusion | flops 2235678720 | bytes 10589696 | tf_op jit(solution)/shard_map/dot_general | solution.py:15
  270.0 35.0 %collective-permute-done = bf16[3,1408,256]{1,2,0:T(8,128)(2,1)} collective-permute-done((bf16[3,1408,256]{1,2,0:T(8,128)(2,1)}, bf16[3,1408,256]{1,2,0:T(8,128)(2,1)}, u32[]{:S(2)}, u32[]{:S(2)}) %collective-permute-start) | collective-permute-done | bytes 2162720 | tf_op jit(solution)/shard_map/ppermute | solution.py:25
  320.1 7.0 %collective-permute-done.6 = bf16[512,384]{1,0:T(8,128)(2,1)} collective-permute-done((bf16[512,384]{1,0:T(8,128)(2,1)}, bf16[512,384]{1,0:T(8,128)(2,1)}, u32[]{:S(2)}, u32[]{:S(2)}) %collective-permute-start.6) | collective-permute-done | bytes 393248 | tf_op jit(solution)/shard_map/ppermute | solution.py:30
  328.9 9.7 %collective-permute-done.8 = bf16[512,384]{1,0:T(8,128)(2,1)S(1)} collective-permute-done((bf16[512,384]{1,0:T(8,128)(2,1)S(1)}, bf16[512,384]{1,0:T(8,128)(2,1)S(1)}, u32[]{:S(2)}, u32[]{:S(2)}) %collective-permute-start.8) | collective-permute-done | bytes 393248 | tf_op jit(solution)/shard_map/ppermute | solution.py:30
  352.1 6.2 all-reduce
  365.2 34.4 %all-gather.27.cloned.1.call-done = bf16[1024,1408]{1,0:T(8,128)(2,1)} async-done(((bf16[256,1408]{1,0:T(8,128)(2,1)}), bf16[1024,1408]{1,0:T(8,128)(2,1)}) %all-gather.27.cloned.1.call-update) | async-done | bytes 2883600 | tf_op jit(solution)/shard_map/all_gather | solution.py:94
  414.0 8.6 %collective-permute-done.11 = bf16[512,384]{1,0:T(8,128)(2,1)S(1)} collective-permute-done((bf16[512,384]{1,0:T(8,128)(2,1)S(1)}, bf16[512,384]{1,0:T(8,128)(2,1)S(1)}, u32[]{:S(2)}, u32[]{:S(2)}) %collective-permute-start.11) | collective-permute-done | bytes 393248 | tf_op jit(solution)/shard_map/ppermute | solution.py:30
  425.3 8.0 %collective-permute-done.14 = bf16[512,384]{1,0:T(8,128)(2,1)S(1)} collective-permute-done((bf16[512,384]{1,0:T(8,128)(2,1)S(1)}, bf16[512,384]{1,0:T(8,128)(2,1)S(1)}, u32[]{:S(2)}, u32[]{:S(2)}) %collective-permute-start.14) | collective-permute-done | bytes 393248 | tf_op jit(solution)/shard_map/ppermute | solution.py:30
  434.3 26.7 %all-gather.29.cloned.1.call-done = bf16[1024,1408]{1,0:T(8,128)(2,1)} async-done(((bf16[256,1408]{1,0:T(8,128)(2,1)}), bf16[1024,1408]{1,0:T(8,128)(2,1)}) %all-gather.29.cloned.1.call-update) | async-done | bytes 2883600 | tf_op jit(solution)/shard_map/all_gather | solution.py:94
  473.2 24.8 %all-gather.31.cloned.1.call-done = bf16[5632,128]{1,0:T(8,128)(2,1)} async-done(((bf16[1408,128]{1,0:T(8,128)(2,1)}), bf16[5632,128]{1,0:T(8,128)(2,1)}) %all-gather.31.cloned.1.call-update) | async-done | bytes 1441808 | tf_op jit(solution)/shard_map/all_gather | solution.py:94
  504.9 9.9 %collective-permute-done.13 = bf16[3,256,1408]{2,1,0:T(8,128)(2,1)} collective-permute-done((bf16[3,256,1408]{2,1,0:T(8,128)(2,1)}, bf16[3,256,1408]{2,1,0:T(8,128)(2,1)}, u32[]{:S(2)}, u32[]{:S(2)}) %collective-permute-start.13) | collective-permute-done | bytes 2162720 | tf_op jit(solution)/shard_map/ppermute | solution.py:25
  514.8 6.3 %fusion.27 = f32[1408,384]{1,0:T(8,128)S(1)} fusion(bf16[2048,384]{1,0:T(8,128)(2,1)} %bitcast_dynamic-update-slice_fusion, bf16[768,1408]{1,0:T(8,128)(2,1)} %bitcast.87, bf16[256,1408]{1,0:T(8,128)(2,1)} %get-tuple-element.73, bf16[1024,1408]{1,0:T(8,128)(2,1)} %all-gather.27.cloned.1.call-done, f32[1408]{0:T(1024)S(1)} %copy-done.38), kind=kOutput, calls=%fused_computation.31 | convolution fusion | flops 2232434688 | bytes 9508352 | tf_op jit(solution)/shard_map/dot_general | solution.py:15
  522.7 38.4 %collective-permute-done.16 = bf16[3,256,1408]{2,1,0:T(8,128)(2,1)} collective-permute-done((bf16[3,256,1408]{2,1,0:T(8,128)(2,1)}, bf16[3,256,1408]{2,1,0:T(8,128)(2,1)}, u32[]{:S(2)}, u32[]{:S(2)}) %collective-permute-start.16) | collective-permute-done | bytes 2162720 | tf_op jit(solution)/shard_map/ppermute | solution.py:25
  561.2 5.6 multiply_convert_fusion.3
  576.5 7.8 %collective-permute-done.12 = bf16[3,1408,128]{1,2,0:T(8,128)(2,1)} collective-permute-done((bf16[3,1408,128]{1,2,0:T(8,128)(2,1)}, bf16[3,1408,128]{1,2,0:T(8,128)(2,1)}, u32[]{:S(2)}, u32[]{:S(2)}) %collective-permute-start.12) | collective-permute-done | bytes 1081376 | tf_op jit(solution)/shard_map/ppermute | solution.py:25
  588.7 17.4 %collective-permute-done.17 = bf16[3,1408,128]{1,2,0:T(8,128)(2,1)S(1)} collective-permute-done((bf16[3,1408,128]{1,2,0:T(8,128)(2,1)S(1)}, bf16[3,1408,128]{1,2,0:T(8,128)(2,1)S(1)}, u32[]{:S(2)}, u32[]{:S(2)}) %collective-permute-start.17) | collective-permute-done | bytes 1081376 | tf_op jit(solution)/shard_map/ppermute | solution.py:25
  612.6 9.7 %collective-permute-done.19 = bf16[512,384]{1,0:T(8,128)(2,1)S(1)} collective-permute-done((bf16[512,384]{1,0:T(8,128)(2,1)S(1)}, bf16[512,384]{1,0:T(8,128)(2,1)S(1)}, u32[]{:S(2)}, u32[]{:S(2)}) %collective-permute-start.19) | collective-permute-done | bytes 393248 | tf_op jit(solution)/shard_map/ppermute | solution.py:30
  (294 shorter events, 150.7 us)
Async XLA Ops:
  6.5 65.3 %all-gather.19.cloned.1.call-start = ((), (), s32[]{:S(2)}) async-start(), calls=%async_computation | async-start | bytes 3604480 | tf_op jit(solution)/shard_map/all_gather | solution.py:94
  9.8 123.3 %all-gather.21.cloned.1.call-start = ((), (), s32[]{:S(2)}) async-start(), calls=%async_computation.1 | async-start | bytes 3604480 | tf_op jit(solution)/shard_map/all_gather | solution.py:94
  75.2 119.5 %all-gather.23.cloned.1.call-start = ((), (), s32[]{:S(2)}) async-start(), calls=%async_computation.2 | async-start | bytes 3604480 | tf_op jit(solution)/shard_map/all_gather | solution.py:94
  136.5 179.5 %all-gather.25.cloned.1.call-start = ((), (), s32[]{:S(2)}) async-start(), calls=%async_computation.3 | async-start | bytes 1966080 | tf_op jit(solution)/shard_map/all_gather | solution.py:94
  136.6 17.0 %collective-permute-start.2 = (bf16[512,384]{1,0:T(8,128)(2,1)S(1)}, bf16[512,384]{1,0:T(8,128)(2,1)}, u32[]{:S(2)}, u32[]{:S(2)}) collective-permute-start(bf16[512,384]{1,0:T(8,128)(2,1)S(1)} %copy-done.6), channel_id=1, source_target_pairs={{0,2},{1,3},{2,0},{3,1},{4,6},{5,7},{6,4},{7,5},{8,10},{9,11},{10,... | collective-permute-start | bytes 1179656 | tf_op jit(solution)/shard_map/ppermute | solution.py:30
  162.5 50.3 %collective-permute-start.1 = (bf16[3,256,1408]{2,1,0:T(8,128)(2,1)}, bf16[3,256,1408]{2,1,0:T(8,128)(2,1)}, u32[]{:S(2)}, u32[]{:S(2)}) collective-permute-start(bf16[3,256,1408]{2,1,0:T(8,128)(2,1)} %pad_maximum_fusion), channel_id=1, source_target_pairs={{0,16},{16,0},{1,17},{17,1},{2,18},{18,2},{3,19},{19,3},{4,20},{20... | collective-permute-start | bytes 6488072 | tf_op jit(solution)/shard_map/ppermute | solution.py:25
  165.4 93.8 %collective-permute-start.4 = (bf16[3,256,1408]{2,1,0:T(8,128)(2,1)}, bf16[3,256,1408]{2,1,0:T(8,128)(2,1)}, u32[]{:S(2)}, u32[]{:S(2)}) collective-permute-start(bf16[3,256,1408]{2,1,0:T(8,128)(2,1)} %pad_maximum_fusion.1), channel_id=1, source_target_pairs={{0,16},{16,0},{1,17},{17,1},{2,18},{18,2},{3,19},{19,3},{4,20},{20... | collective-permute-start | bytes 6488072 | tf_op jit(solution)/shard_map/ppermute | solution.py:25
  207.8 97.2 %collective-permute-start = (bf16[3,1408,256]{1,2,0:T(8,128)(2,1)}, bf16[3,1408,256]{1,2,0:T(8,128)(2,1)}, u32[]{:S(2)}, u32[]{:S(2)}) collective-permute-start(bf16[3,1408,256]{1,2,0:T(8,128)(2,1)} %pad_maximum_fusion.2), channel_id=1, source_target_pairs={{0,16},{16,0},{1,17},{17,1},{2,18},{18,2},{3,19},{19,3},{4,20},{20... | collective-permute-start | bytes 6488072 | tf_op jit(solution)/shard_map/ppermute | solution.py:25
  265.8 133.8 %all-gather.27.cloned.1.call-start = ((), (), s32[]{:S(2)}) async-start(), calls=%async_computation.4 | async-start | bytes 3604480 | tf_op jit(solution)/shard_map/all_gather | solution.py:94
  315.5 11.5 %collective-permute-start.6 = (bf16[512,384]{1,0:T(8,128)(2,1)}, bf16[512,384]{1,0:T(8,128)(2,1)}, u32[]{:S(2)}, u32[]{:S(2)}) collective-permute-start(bf16[512,384]{1,0:T(8,128)(2,1)} %fusion.98), channel_id=1, source_target_pairs={{0,2},{1,3},{2,0},{3,1},{4,6},{5,7},{6,4},{7,5},{8,10},{9,11},{10,... | collective-permute-start | bytes 1179656 | tf_op jit(solution)/shard_map/ppermute | solution.py:30
  318.6 28.0 %collective-permute-start.7 = (bf16[3,3,256,256]{3,2,0,1:T(8,128)(2,1)}, bf16[3,3,256,256]{3,2,0,1:T(8,128)(2,1)}, u32[]{:S(2)}, u32[]{:S(2)}) collective-permute-start(bf16[3,3,256,256]{3,2,0,1:T(8,128)(2,1)} %pad_maximum_fusion.5), channel_id=1, source_target_pairs={{0,16},{16,0},{1,17},{17,1},{2,18},{18,2},{3,19},{19,3},{4,20},{20... | collective-permute-start | bytes 3538952 | tf_op jit(solution)/shard_map/ppermute | solution.py:25
  328.2 10.4 %collective-permute-start.8 = (bf16[512,384]{1,0:T(8,128)(2,1)S(1)}, bf16[512,384]{1,0:T(8,128)(2,1)S(1)}, u32[]{:S(2)}, u32[]{:S(2)}) collective-permute-start(bf16[512,384]{1,0:T(8,128)(2,1)S(1)} %fusion.73), channel_id=1, source_target_pairs={{0,2},{1,3},{2,0},{3,1},{4,6},{5,7},{6,4},{7,5},{8,10},{9,11},{10,... | collective-permute-start | bytes 1179656 | tf_op jit(solution)/shard_map/ppermute | solution.py:30
  339.5 8.3 %collective-permute-start.9 = (bf16[2,512,384]{2,1,0:T(8,128)(2,1)}, bf16[2,512,384]{2,1,0:T(8,128)(2,1)}, u32[]{:S(2)}, u32[]{:S(2)}) collective-permute-start(bf16[2,512,384]{2,1,0:T(8,128)(2,1)} %pad_maximum_fusion.9), channel_id=1, source_target_pairs={{0,1},{1,0},{2,3},{3,2},{4,5},{5,4},{6,7},{7,6},{8,9},{9,8},{10,11... | collective-permute-start | bytes 2359304 | tf_op jit(solution)/shard_map/ppermute | solution.py:36
  342.7 118.3 %all-gather.29.cloned.1.call-start = ((), (), s32[]{:S(2)}) async-start(), calls=%async_computation.5 | async-start | bytes 3604480 | tf_op jit(solution)/shard_map/all_gather | solution.py:94
  403.1 94.9 %all-gather.31.cloned.1.call-start = ((), (), s32[]{:S(2)}) async-start(), calls=%async_computation.6 | async-start | bytes 1802240 | tf_op jit(solution)/shard_map/all_gather | solution.py:94
  411.4 11.2 %collective-permute-start.11 = (bf16[512,384]{1,0:T(8,128)(2,1)S(1)}, bf16[512,384]{1,0:T(8,128)(2,1)S(1)}, u32[]{:S(2)}, u32[]{:S(2)}) collective-permute-start(bf16[512,384]{1,0:T(8,128)(2,1)S(1)} %fusion.99), channel_id=1, source_target_pairs={{0,2},{1,3},{2,0},{3,1},{4,6},{5,7},{6,4},{7,5},{8,10},{9,11},{10,... | collective-permute-start | bytes 1179656 | tf_op jit(solution)/shard_map/ppermute | solution.py:30
  422.8 10.5 %collective-permute-start.14 = (bf16[512,384]{1,0:T(8,128)(2,1)S(1)}, bf16[512,384]{1,0:T(8,128)(2,1)S(1)}, u32[]{:S(2)}, u32[]{:S(2)}) collective-permute-start(bf16[512,384]{1,0:T(8,128)(2,1)S(1)} %fusion.70), channel_id=1, source_target_pairs={{0,2},{1,3},{2,0},{3,1},{4,6},{5,7},{6,4},{7,5},{8,10},{9,11},{10,... | collective-permute-start | bytes 1179656 | tf_op jit(solution)/shard_map/ppermute | solution.py:30
  434.3 31.8 %collective-permute-start.15 = (bf16[2,512,384]{2,1,0:T(8,128)(2,1)}, bf16[2,512,384]{2,1,0:T(8,128)(2,1)}, u32[]{:S(2)}, u32[]{:S(2)}) collective-permute-start(bf16[2,512,384]{2,1,0:T(8,128)(2,1)} %pad_maximum_fusion.10), channel_id=1, source_target_pairs={{0,1},{1,0},{2,3},{3,2},{4,5},{5,4},{6,7},{7,6},{8,9},{9,8},{10,11... | collective-permute-start | bytes 2359304 | tf_op jit(solution)/shard_map/ppermute | solution.py:36
  464.4 102.4 %all-gather.33.cloned.1.call-start = ((), (), s32[]{:S(2)}) async-start(), calls=%async_computation.7 | async-start | bytes 1802240 | tf_op jit(solution)/shard_map/all_gather | solution.py:94
  464.5 50.3 %collective-permute-start.13 = (bf16[3,256,1408]{2,1,0:T(8,128)(2,1)}, bf16[3,256,1408]{2,1,0:T(8,128)(2,1)}, u32[]{:S(2)}, u32[]{:S(2)}) collective-permute-start(bf16[3,256,1408]{2,1,0:T(8,128)(2,1)} %pad_maximum_fusion.3), channel_id=1, source_target_pairs={{0,16},{16,0},{1,17},{17,1},{2,18},{18,2},{3,19},{19,3},{4,20},{20... | collective-permute-start | bytes 6488072 | tf_op jit(solution)/shard_map/ppermute | solution.py:25
  469.1 92.0 %collective-permute-start.16 = (bf16[3,256,1408]{2,1,0:T(8,128)(2,1)}, bf16[3,256,1408]{2,1,0:T(8,128)(2,1)}, u32[]{:S(2)}, u32[]{:S(2)}) collective-permute-start(bf16[3,256,1408]{2,1,0:T(8,128)(2,1)} %pad_maximum_fusion.4), channel_id=1, source_target_pairs={{0,16},{16,0},{1,17},{17,1},{2,18},{18,2},{3,19},{19,3},{4,20},{20... | collective-permute-start | bytes 6488072 | tf_op jit(solution)/shard_map/ppermute | solution.py:25
  521.2 63.1 %collective-permute-start.12 = (bf16[3,1408,128]{1,2,0:T(8,128)(2,1)}, bf16[3,1408,128]{1,2,0:T(8,128)(2,1)}, u32[]{:S(2)}, u32[]{:S(2)}) collective-permute-start(bf16[3,1408,128]{1,2,0:T(8,128)(2,1)} %pad_maximum_fusion.6), channel_id=1, source_target_pairs={{0,16},{16,0},{1,17},{17,1},{2,18},{18,2},{3,19},{19,3},{4,20},{20... | collective-permute-start | bytes 3244040 | tf_op jit(solution)/shard_map/ppermute | solution.py:25
  574.0 32.1 %collective-permute-start.17 = (bf16[3,1408,128]{1,2,0:T(8,128)(2,1)S(1)}, bf16[3,1408,128]{1,2,0:T(8,128)(2,1)S(1)}, u32[]{:S(2)}, u32[]{:S(2)}) collective-permute-start(bf16[3,1408,128]{1,2,0:T(8,128)(2,1)S(1)} %pad_maximum_fusion.7), channel_id=1, source_target_pairs={{0,16},{16,0},{1,17},{17,1},{2,18},{18,2},{3,19},{19,3},{4,20},{20... | collective-permute-start | bytes 3244040 | tf_op jit(solution)/shard_map/ppermute | solution.py:25
  611.1 11.2 %collective-permute-start.19 = (bf16[512,384]{1,0:T(8,128)(2,1)S(1)}, bf16[512,384]{1,0:T(8,128)(2,1)S(1)}, u32[]{:S(2)}, u32[]{:S(2)}) collective-permute-start(bf16[512,384]{1,0:T(8,128)(2,1)S(1)} %fusion.100), channel_id=1, source_target_pairs={{0,2},{1,3},{2,0},{3,1},{4,6},{5,7},{6,4},{7,5},{8,10},{9,11},{10,... | collective-permute-start | bytes 1179656 | tf_op jit(solution)/shard_map/ppermute | solution.py:30
  (47 other events, 679.0 us)
Sparse Core Ops, SparseCore 0:
  10.0 61.8 all-gather.18
  75.3 57.7 all-gather.20
  136.6 58.0 all-gather.22
  265.9 34.5 all-gather.24
  342.9 56.6 all-gather.26
  403.2 57.7 all-gather.28
  464.5 33.4 all-gather.30
  503.6 33.7 all-gather.32

commit v2 on v1

--- a/solution.py
+++ b/solution.py
@@ -65,7 +65,7 @@
     return jnp.concatenate(found)
 
 
-def scatter_sum(terms):
+def scatter_blocks(terms):
     chips = lax.axis_size("tp") // CORES
     chip, core = chip_and_core()
     blocks = terms.reshape((chips, CORES, -1) + terms.shape[1:])
@@ -255,10 +255,10 @@
         return cut
 
     units = (
+        mixer_share,
         rows_share(first_gate),
         rows_share(first_up),
         cols_share(first_down, 0, 1),
-        mixer_share,
         rows_share(second_gate),
         rows_share(second_up),
     ) + tuple(cols_share(second_down, part, LAST_PARTS) for part in range(LAST_PARTS))
@@ -284,13 +284,13 @@
         ordered = [
             term[at][share] for at in range(count) for share in range(shares) for term in terms
         ]
-        return residual(stream, scatter_sum(jnp.concatenate(ordered)), 0.5)
+        return residual(stream, scatter_blocks(jnp.concatenate(ordered)), 0.5)
 
     stream = half_step(
-        stream, first_gain, ready[0], first_gate_scale, ready[1], first_up_scale, ready[2:3], cols[:, 0]
+        stream, first_gain, ready[1], first_gate_scale, ready[2], first_up_scale, ready[3:4], cols[:, 0]
     )
     rows = rows_in_order(normed(stream, mixer_gain))
-    blocks, rests, local_shares = ready[3]
+    blocks, rests, local_shares = ready[0]
 
     def mixer_unit(index):
         return (
@@ -310,7 +310,7 @@
     )
     terms = column_terms(*mixer_unit(2), cols[:, 1], gated, True)
     terms = jnp.concatenate([terms[at][share] for at in range(count) for share in range(shares)])
-    stream = residual(stream, scatter_sum(terms), 1.0)
+    stream = residual(stream, scatter_blocks(terms), 1.0)
     return half_step(
         stream, second_gain, ready[4], second_gate_scale, ready[5], second_up_scale, ready[6:], cols[:, 2]
     )

time: 640 us -> 631 us (0.986)
  waiting for transfers between devices: 430 us -> 420 us
  other arithmetic: 40.7 us -> 34 us
  local copies, waits for them, and re-layouts: 63.2 us -> 69.9 us
    all_gather x8, waiting for transfers between devices: 224 us -> 200 us  [exchange(): blocks = lax.all_gather(share, 'fs', axis=0, tiled=False)]
    ppermute x8, waiting for transfers between devices: 157 us -> 165 us  [shifted(): lax.ppermute(block, axis_name, [(at, (at + step) % count) for at in range...]
    unnamed x124 -> x126, local copies, waits for them, and re-layouts: 29.2 us -> 32.1 us
  transfers between devices with their start and end apart: 28 -> 28, of which waited for: 22 -> 23; matrix products, arithmetic and copies ran while one was open for 20% -> 20% of each run, Pallas kernels for 0% -> 0%
where the time goes in v2:
time: 631 us; the launch traced here: 622 us
  waiting for transfers between devices  420 us (67%)
  local copies, waits for them, and re-layouts  69.9 us (11%)
  matrix products  44.3 us (7%)
  other arithmetic  34 us (5%)
  blocking collectives  20.7 us (3%)
  starting transfers between devices  18 us (3%)
  between operations  14.7 us (2%)
    all_gather x8, waiting for transfers between devices, exchange(): blocks = lax.all_gather(share, 'fs', axis=0, tiled=False)  200 us
    ppermute x8, waiting for transfers between devices, shifted(): lax.ppermute(block, axis_name, [(at, (at + step) % count) for at in range...  165 us
    ppermute x6, waiting for transfers between devices, to_same_core(): lax.ppermute(block, 'tp', [(at, (at + step * CORES) % count) for at in ra...  48.7 us
    unnamed x126, local copies, waits for them, and re-layouts  32.1 us
    dot_general x6, matrix products, contract(): lax.dot_general(left_side, right_side, (((0,), (0,)), ((), ())), preferre...  26.7 us
    dot_general x12, matrix products, product(): return jnp.einsum(form, pieces, hidden, preferred_element_type=jnp.float32)  17.3 us
    another operation x8, other arithmetic, exchange(): jnp.stack([lax.dynamic_index_in_dim(blocks, ring_place(step), 0, keepdims...  14.4 us
    all_gather x1, blocking collectives, layer(): lax.all_gather(jnp.stack([first_down_scale, mixer_out_scale, second_down_...  14.4 us
  transfers between devices with their start and end apart: 28, of which 23 were waited for; matrix products, arithmetic and copies ran while one was open for 20% of the time, Pallas kernels for 0%

profile of v2, /device:TPU:0, one launch (start us, length us, event | category | flops | bytes accessed | tf_op | source)
XLA Modules:
  0.0 621.9 jit_solution(4345857847460827342)
XLA Ops:
  14.2 35.5 %all-gather.19.cloned.1.call-done = bf16[12,256,256]{2,1,0:T(8,128)(2,1)} async-done(((bf16[3,256,256]{2,1,0:T(8,128)(2,1)}), bf16[12,256,256]{2,1,0:T(8,128)(2,1)}) %all-gather.19.cloned.1.call-update) | async-done | bytes 1572880 | tf_op jit(solution)/shard_map/all_gather | solution.py:94
  55.4 55.0 %all-gather.21.cloned.1.call-done = bf16[1024,1408]{1,0:T(8,128)(2,1)} async-done(((bf16[256,1408]{1,0:T(8,128)(2,1)}), bf16[1024,1408]{1,0:T(8,128)(2,1)}) %all-gather.21.cloned.1.call-update) | async-done | bytes 2883600 | tf_op jit(solution)/shard_map/all_gather | solution.py:94
  114.8 56.9 %all-gather.23.cloned.1.call-done = bf16[1024,1408]{1,0:T(8,128)(2,1)} async-done(((bf16[256,1408]{1,0:T(8,128)(2,1)}), bf16[1024,1408]{1,0:T(8,128)(2,1)}) %all-gather.23.cloned.1.call-update) | async-done | bytes 2883600 | tf_op jit(solution)/shard_map/all_gather | solution.py:94
  176.7 9.2 %collective-permute-done.2 = bf16[512,384]{1,0:T(8,128)(2,1)S(1)} collective-permute-done((bf16[512,384]{1,0:T(8,128)(2,1)S(1)}, bf16[512,384]{1,0:T(8,128)(2,1)S(1)}, u32[]{:S(2)}, u32[]{:S(2)}) %collective-permute-start.2) | collective-permute-done | bytes 393248 | tf_op jit(solution)/shard_map/ppermute | solution.py:30
  188.4 14.4 %all-gather.9 = f32[4,3,512]{2,1,0:T(4,128)} all-gather(f32[1,3,512]{2,1,0:T(4,128)S(1)} %maximum_bitcast_fusion), channel_id=6, replica_groups=mesh['grp'=2,'fs'=4,'tp'=4] {'fs'}, dimensions={0}, use_global_device_ids=true | all-gather | bytes 30720 | tf_op jit(solution)/shard_map/all_gather | solution.py:232
  218.9 14.6 %all-gather.25.cloned.1.call-done = bf16[5632,256]{1,0:T(8,128)(2,1)} async-done(((bf16[1408,256]{1,0:T(8,128)(2,1)}), bf16[5632,256]{1,0:T(8,128)(2,1)}) %all-gather.25.cloned.1.call-update) | async-done | bytes 2883600 | tf_op jit(solution)/shard_map/all_gather | solution.py:94
  247.9 12.9 %collective-permute-done.1 = bf16[3,256,1408]{2,1,0:T(8,128)(2,1)} collective-permute-done((bf16[3,256,1408]{2,1,0:T(8,128)(2,1)}, bf16[3,256,1408]{2,1,0:T(8,128)(2,1)}, u32[]{:S(2)}, u32[]{:S(2)}) %collective-permute-start.1) | collective-permute-done | bytes 2162720 | tf_op jit(solution)/shard_map/ppermute | solution.py:25
  260.8 6.3 %fusion.33 = f32[1408,384]{1,0:T(8,128)S(1)} fusion(bf16[2048,384]{1,0:T(8,128)(2,1)} %bitcast_dynamic-update-slice_fusion.16, bf16[768,1408]{1,0:T(8,128)(2,1)} %bitcast.8, bf16[256,1408]{1,0:T(8,128)(2,1)} %get-tuple-element.154, bf16[1024,1408]{1,0:T(8,128)(2,1)} %all-gather.21.cloned.1.call-done, f32[1408]{0:T(1024)S(1)} %copy-done.37), kind=kOutput, calls=%fused_computation.33 | convolution fusion | flops 2232434688 | bytes 9508352 | tf_op jit(solution)/shard_map/dot_general | solution.py:15
  267.1 40.0 %collective-permute-done.4 = bf16[3,256,1408]{2,1,0:T(8,128)(2,1)} collective-permute-done((bf16[3,256,1408]{2,1,0:T(8,128)(2,1)}, bf16[3,256,1408]{2,1,0:T(8,128)(2,1)}, u32[]{:S(2)}, u32[]{:S(2)}) %collective-permute-start.4) | collective-permute-done | bytes 2162720 | tf_op jit(solution)/shard_map/ppermute | solution.py:25
  307.2 6.6 %multiply_convert_fusion.4 = bf16[1408,384]{1,0:T(8,128)(2,1)} fusion(f32[1408,384]{1,0:T(8,128)S(1)} %fusion.33, f32[1408]{0:T(1024)S(1)} %copy-done.38, bf16[2048,384]{1,0:T(8,128)(2,1)} %bitcast_dynamic-update-slice_fusion.16, bf16[768,1408]{1,0:T(8,128)(2,1)} %bitcast.22, bf16[256,1408]{1,0:T(8,128)(2,1)S(1)} %copy-done.13, ...), kind=kOutput, calls=%fused_computation.40 | convolution fusion | flops 2235678720 | bytes 10589696 | tf_op jit(solution)/shard_map/dot_general | solution.py:15
  318.3 32.1 %collective-permute-done = bf16[3,1408,256]{1,2,0:T(8,128)(2,1)} collective-permute-done((bf16[3,1408,256]{1,2,0:T(8,128)(2,1)}, bf16[3,1408,256]{1,2,0:T(8,128)(2,1)}, u32[]{:S(2)}, u32[]{:S(2)}) %collective-permute-start) | collective-permute-done | bytes 2162720 | tf_op jit(solution)/shard_map/ppermute | solution.py:25
  365.2 6.3 %collective-permute-done.6 = bf16[512,384]{1,0:T(8,128)(2,1)S(1)} collective-permute-done((bf16[512,384]{1,0:T(8,128)(2,1)S(1)}, bf16[512,384]{1,0:T(8,128)(2,1)S(1)}, u32[]{:S(2)}, u32[]{:S(2)}) %collective-permute-start.6) | collective-permute-done | bytes 393248 | tf_op jit(solution)/shard_map/ppermute | solution.py:30
  383.2 6.8 %collective-permute-done.7 = bf16[3,3,256,256]{3,2,0,1:T(8,128)(2,1)} collective-permute-done((bf16[3,3,256,256]{3,2,0,1:T(8,128)(2,1)}, bf16[3,3,256,256]{3,2,0,1:T(8,128)(2,1)}, u32[]{:S(2)}, u32[]{:S(2)}) %collective-permute-start.7) | collective-permute-done | bytes 1179680 | tf_op jit(solution)/shard_map/ppermute | solution.py:25
  400.0 6.3 %all-reduce = (f32[384]{0:T(512)S(1)}, f32[384]{0:T(512)S(1)}) all-reduce(f32[384]{0:T(512)S(1)} %get-tuple-element.34, f32[384]{0:T(512)S(1)} %get-tuple-element.33), channel_id=1, replica_groups=mesh['grp'=2,'fs'=4,'tp'=4] {'tp'}, use_global_device_ids=true, to_apply=%region_5.6 | all-reduce | flops 768 | bytes 6144 | tf_op jit(solution)/shard_map/psum | solution.py:188
  419.1 8.7 %collective-permute-done.11 = bf16[512,384]{1,0:T(8,128)(2,1)S(1)} collective-permute-done((bf16[512,384]{1,0:T(8,128)(2,1)S(1)}, bf16[512,384]{1,0:T(8,128)(2,1)S(1)}, u32[]{:S(2)}, u32[]{:S(2)}) %collective-permute-start.11) | collective-permute-done | bytes 393248 | tf_op jit(solution)/shard_map/ppermute | solution.py:30
  429.3 9.2 %collective-permute-done.14 = bf16[512,384]{1,0:T(8,128)(2,1)S(1)} collective-permute-done((bf16[512,384]{1,0:T(8,128)(2,1)S(1)}, bf16[512,384]{1,0:T(8,128)(2,1)S(1)}, u32[]{:S(2)}, u32[]{:S(2)}) %collective-permute-start.14) | collective-permute-done | bytes 393248 | tf_op jit(solution)/shard_map/ppermute | solution.py:30
  439.5 13.1 %all-gather.29.cloned.1.call-done = bf16[1024,1408]{1,0:T(8,128)(2,1)} async-done(((bf16[256,1408]{1,0:T(8,128)(2,1)}), bf16[1024,1408]{1,0:T(8,128)(2,1)}) %all-gather.29.cloned.1.call-update) | async-done | bytes 2883600 | tf_op jit(solution)/shard_map/all_gather | solution.py:94
  464.8 24.8 %all-gather.31.cloned.1.call-done = bf16[5632,128]{1,0:T(8,128)(2,1)} async-done(((bf16[1408,128]{1,0:T(8,128)(2,1)}), bf16[5632,128]{1,0:T(8,128)(2,1)}) %all-gather.31.cloned.1.call-update) | async-done | bytes 1441808 | tf_op jit(solution)/shard_map/all_gather | solution.py:94
  496.5 9.9 %collective-permute-done.13 = bf16[3,256,1408]{2,1,0:T(8,128)(2,1)} collective-permute-done((bf16[3,256,1408]{2,1,0:T(8,128)(2,1)}, bf16[3,256,1408]{2,1,0:T(8,128)(2,1)}, u32[]{:S(2)}, u32[]{:S(2)}) %collective-permute-start.13) | collective-permute-done | bytes 2162720 | tf_op jit(solution)/shard_map/ppermute | solution.py:25
  506.4 6.6 %fusion.27 = f32[1408,384]{1,0:T(8,128)S(1)} fusion(bf16[2048,384]{1,0:T(8,128)(2,1)} %bitcast_dynamic-update-slice_fusion, bf16[768,1408]{1,0:T(8,128)(2,1)} %bitcast.87, bf16[256,1408]{1,0:T(8,128)(2,1)} %get-tuple-element.73, bf16[1024,1408]{1,0:T(8,128)(2,1)} %all-gather.27.cloned.1.call-done, f32[1408]{0:T(1024)S(1)} %copy-done.39), kind=kOutput, calls=%fused_computation.31 | convolution fusion | flops 2232434688 | bytes 9508352 | tf_op jit(solution)/shard_map/dot_general | solution.py:15
  514.5 38.2 %collective-permute-done.16 = bf16[3,256,1408]{2,1,0:T(8,128)(2,1)} collective-permute-done((bf16[3,256,1408]{2,1,0:T(8,128)(2,1)}, bf16[3,256,1408]{2,1,0:T(8,128)(2,1)}, u32[]{:S(2)}, u32[]{:S(2)}) %collective-permute-start.16) | collective-permute-done | bytes 2162720 | tf_op jit(solution)/shard_map/ppermute | solution.py:25
  568.1 7.8 %collective-permute-done.12 = bf16[3,1408,128]{1,2,0:T(8,128)(2,1)} collective-permute-done((bf16[3,1408,128]{1,2,0:T(8,128)(2,1)}, bf16[3,1408,128]{1,2,0:T(8,128)(2,1)}, u32[]{:S(2)}, u32[]{:S(2)}) %collective-permute-start.12) | collective-permute-done | bytes 1081376 | tf_op jit(solution)/shard_map/ppermute | solution.py:25
  580.3 17.4 %collective-permute-done.17 = bf16[3,1408,128]{1,2,0:T(8,128)(2,1)S(1)} collective-permute-done((bf16[3,1408,128]{1,2,0:T(8,128)(2,1)S(1)}, bf16[3,1408,128]{1,2,0:T(8,128)(2,1)S(1)}, u32[]{:S(2)}, u32[]{:S(2)}) %collective-permute-start.17) | collective-permute-done | bytes 1081376 | tf_op jit(solution)/shard_map/ppermute | solution.py:25
  604.2 9.7 %collective-permute-done.19 = bf16[512,384]{1,0:T(8,128)(2,1)S(1)} collective-permute-done((bf16[512,384]{1,0:T(8,128)(2,1)S(1)}, bf16[512,384]{1,0:T(8,128)(2,1)S(1)}, u32[]{:S(2)}, u32[]{:S(2)}) %collective-permute-start.19) | collective-permute-done | bytes 393248 | tf_op jit(solution)/shard_map/ppermute | solution.py:30
  (296 shorter events, 158.8 us)
Async XLA Ops:
  6.5 43.2 %all-gather.19.cloned.1.call-start = ((), (), s32[]{:S(2)}) async-start(), calls=%async_computation | async-start | bytes 1966080 | tf_op jit(solution)/shard_map/all_gather | solution.py:94
  9.8 100.6 %all-gather.21.cloned.1.call-start = ((), (), s32[]{:S(2)}) async-start(), calls=%async_computation.1 | async-start | bytes 3604480 | tf_op jit(solution)/shard_map/all_gather | solution.py:94
  52.3 119.5 %all-gather.23.cloned.1.call-start = ((), (), s32[]{:S(2)}) async-start(), calls=%async_computation.2 | async-start | bytes 3604480 | tf_op jit(solution)/shard_map/all_gather | solution.py:94
  113.8 119.7 %all-gather.25.cloned.1.call-start = ((), (), s32[]{:S(2)}) async-start(), calls=%async_computation.3 | async-start | bytes 3604480 | tf_op jit(solution)/shard_map/all_gather | solution.py:94
  175.1 216.9 %all-gather.27.cloned.1.call-start = ((), (), s32[]{:S(2)}) async-start(), calls=%async_computation.4 | async-start | bytes 3604480 | tf_op jit(solution)/shard_map/all_gather | solution.py:94
  175.2 10.8 %collective-permute-start.2 = (bf16[512,384]{1,0:T(8,128)(2,1)S(1)}, bf16[512,384]{1,0:T(8,128)(2,1)S(1)}, u32[]{:S(2)}, u32[]{:S(2)}) collective-permute-start(bf16[512,384]{1,0:T(8,128)(2,1)S(1)} %copy-done.5), channel_id=1, source_target_pairs={{0,2},{1,3},{2,0},{3,1},{4,6},{5,7},{6,4},{7,5},{8,10},{9,11},{10,... | collective-permute-start | bytes 1179656 | tf_op jit(solution)/shard_map/ppermute | solution.py:30
  187.7 20.9 %collective-permute-start.3 = (bf16[2,512,384]{2,1,0:T(8,128)(2,1)}, bf16[2,512,384]{2,1,0:T(8,128)(2,1)}, u32[]{:S(2)}, u32[]{:S(2)}) collective-permute-start(bf16[2,512,384]{2,1,0:T(8,128)(2,1)} %pad_maximum_fusion.8), channel_id=1, source_target_pairs={{0,1},{1,0},{2,3},{3,2},{4,5},{5,4},{6,7},{7,6},{8,9},{9,8},{10,11... | collective-permute-start | bytes 2359304 | tf_op jit(solution)/shard_map/ppermute | solution.py:36
  210.5 50.3 %collective-permute-start.1 = (bf16[3,256,1408]{2,1,0:T(8,128)(2,1)}, bf16[3,256,1408]{2,1,0:T(8,128)(2,1)}, u32[]{:S(2)}, u32[]{:S(2)}) collective-permute-start(bf16[3,256,1408]{2,1,0:T(8,128)(2,1)} %pad_maximum_fusion), channel_id=1, source_target_pairs={{0,16},{16,0},{1,17},{17,1},{2,18},{18,2},{3,19},{19,3},{4,20},{20... | collective-permute-start | bytes 6488072 | tf_op jit(solution)/shard_map/ppermute | solution.py:25
  213.4 93.8 %collective-permute-start.4 = (bf16[3,256,1408]{2,1,0:T(8,128)(2,1)}, bf16[3,256,1408]{2,1,0:T(8,128)(2,1)}, u32[]{:S(2)}, u32[]{:S(2)}) collective-permute-start(bf16[3,256,1408]{2,1,0:T(8,128)(2,1)} %pad_maximum_fusion.1), channel_id=1, source_target_pairs={{0,16},{16,0},{1,17},{17,1},{2,18},{18,2},{3,19},{19,3},{4,20},{20... | collective-permute-start | bytes 6488072 | tf_op jit(solution)/shard_map/ppermute | solution.py:25
  246.4 103.9 %collective-permute-start = (bf16[3,1408,256]{1,2,0:T(8,128)(2,1)}, bf16[3,1408,256]{1,2,0:T(8,128)(2,1)}, u32[]{:S(2)}, u32[]{:S(2)}) collective-permute-start(bf16[3,1408,256]{1,2,0:T(8,128)(2,1)} %pad_maximum_fusion.2), channel_id=1, source_target_pairs={{0,16},{16,0},{1,17},{17,1},{2,18},{18,2},{3,19},{19,3},{4,20},{20... | collective-permute-start | bytes 6488072 | tf_op jit(solution)/shard_map/ppermute | solution.py:25
  313.8 138.9 %all-gather.29.cloned.1.call-start = ((), (), s32[]{:S(2)}) async-start(), calls=%async_computation.5 | async-start | bytes 3604480 | tf_op jit(solution)/shard_map/all_gather | solution.py:94
  360.3 11.2 %collective-permute-start.6 = (bf16[512,384]{1,0:T(8,128)(2,1)S(1)}, bf16[512,384]{1,0:T(8,128)(2,1)S(1)}, u32[]{:S(2)}, u32[]{:S(2)}) collective-permute-start(bf16[512,384]{1,0:T(8,128)(2,1)S(1)} %fusion.98), channel_id=1, source_target_pairs={{0,2},{1,3},{2,0},{3,1},{4,6},{5,7},{6,4},{7,5},{8,10},{9,11},{10,... | collective-permute-start | bytes 1179656 | tf_op jit(solution)/shard_map/ppermute | solution.py:30
  361.8 28.1 %collective-permute-start.7 = (bf16[3,3,256,256]{3,2,0,1:T(8,128)(2,1)}, bf16[3,3,256,256]{3,2,0,1:T(8,128)(2,1)}, u32[]{:S(2)}, u32[]{:S(2)}) collective-permute-start(bf16[3,3,256,256]{3,2,0,1:T(8,128)(2,1)} %pad_maximum_fusion.5), channel_id=1, source_target_pairs={{0,16},{16,0},{1,17},{17,1},{2,18},{18,2},{3,19},{19,3},{4,20},{20... | collective-permute-start | bytes 3538952 | tf_op jit(solution)/shard_map/ppermute | solution.py:25
  371.7 10.5 %collective-permute-start.8 = (bf16[512,384]{1,0:T(8,128)(2,1)S(1)}, bf16[512,384]{1,0:T(8,128)(2,1)S(1)}, u32[]{:S(2)}, u32[]{:S(2)}) collective-permute-start(bf16[512,384]{1,0:T(8,128)(2,1)S(1)} %fusion.73), channel_id=1, source_target_pairs={{0,2},{1,3},{2,0},{3,1},{4,6},{5,7},{6,4},{7,5},{8,10},{9,11},{10,... | collective-permute-start | bytes 1179656 | tf_op jit(solution)/shard_map/ppermute | solution.py:30
  383.2 12.3 %collective-permute-start.9 = (bf16[2,512,384]{2,1,0:T(8,128)(2,1)}, bf16[2,512,384]{2,1,0:T(8,128)(2,1)}, u32[]{:S(2)}, u32[]{:S(2)}) collective-permute-start(bf16[2,512,384]{2,1,0:T(8,128)(2,1)} %pad_maximum_fusion.9), channel_id=1, source_target_pairs={{0,1},{1,0},{2,3},{3,2},{4,5},{5,4},{6,7},{7,6},{8,9},{9,8},{10,11... | collective-permute-start | bytes 2359304 | tf_op jit(solution)/shard_map/ppermute | solution.py:36
  395.5 94.1 %all-gather.31.cloned.1.call-start = ((), (), s32[]{:S(2)}) async-start(), calls=%async_computation.6 | async-start | bytes 1802240 | tf_op jit(solution)/shard_map/all_gather | solution.py:94
  416.6 11.2 %collective-permute-start.11 = (bf16[512,384]{1,0:T(8,128)(2,1)S(1)}, bf16[512,384]{1,0:T(8,128)(2,1)S(1)}, u32[]{:S(2)}, u32[]{:S(2)}) collective-permute-start(bf16[512,384]{1,0:T(8,128)(2,1)S(1)} %fusion.99), channel_id=1, source_target_pairs={{0,2},{1,3},{2,0},{3,1},{4,6},{5,7},{6,4},{7,5},{8,10},{9,11},{10,... | collective-permute-start | bytes 1179656 | tf_op jit(solution)/shard_map/ppermute | solution.py:30
  439.5 18.2 %collective-permute-start.15 = (bf16[2,512,384]{2,1,0:T(8,128)(2,1)}, bf16[2,512,384]{2,1,0:T(8,128)(2,1)}, u32[]{:S(2)}, u32[]{:S(2)}) collective-permute-start(bf16[2,512,384]{2,1,0:T(8,128)(2,1)} %pad_maximum_fusion.10), channel_id=1, source_target_pairs={{0,1},{1,0},{2,3},{3,2},{4,5},{5,4},{6,7},{7,6},{8,9},{9,8},{10,11... | collective-permute-start | bytes 2359304 | tf_op jit(solution)/shard_map/ppermute | solution.py:36
  456.0 102.4 %all-gather.33.cloned.1.call-start = ((), (), s32[]{:S(2)}) async-start(), calls=%async_computation.7 | async-start | bytes 1802240 | tf_op jit(solution)/shard_map/all_gather | solution.py:94
  456.1 50.3 %collective-permute-start.13 = (bf16[3,256,1408]{2,1,0:T(8,128)(2,1)}, bf16[3,256,1408]{2,1,0:T(8,128)(2,1)}, u32[]{:S(2)}, u32[]{:S(2)}) collective-permute-start(bf16[3,256,1408]{2,1,0:T(8,128)(2,1)} %pad_maximum_fusion.3), channel_id=1, source_target_pairs={{0,16},{16,0},{1,17},{17,1},{2,18},{18,2},{3,19},{19,3},{4,20},{20... | collective-permute-start | bytes 6488072 | tf_op jit(solution)/shard_map/ppermute | solution.py:25
  460.7 92.0 %collective-permute-start.16 = (bf16[3,256,1408]{2,1,0:T(8,128)(2,1)}, bf16[3,256,1408]{2,1,0:T(8,128)(2,1)}, u32[]{:S(2)}, u32[]{:S(2)}) collective-permute-start(bf16[3,256,1408]{2,1,0:T(8,128)(2,1)} %pad_maximum_fusion.4), channel_id=1, source_target_pairs={{0,16},{16,0},{1,17},{17,1},{2,18},{18,2},{3,19},{19,3},{4,20},{20... | collective-permute-start | bytes 6488072 | tf_op jit(solution)/shard_map/ppermute | solution.py:25
  513.0 62.9 %collective-permute-start.12 = (bf16[3,1408,128]{1,2,0:T(8,128)(2,1)}, bf16[3,1408,128]{1,2,0:T(8,128)(2,1)}, u32[]{:S(2)}, u32[]{:S(2)}) collective-permute-start(bf16[3,1408,128]{1,2,0:T(8,128)(2,1)} %pad_maximum_fusion.6), channel_id=1, source_target_pairs={{0,16},{16,0},{1,17},{17,1},{2,18},{18,2},{3,19},{19,3},{4,20},{20... | collective-permute-start | bytes 3244040 | tf_op jit(solution)/shard_map/ppermute | solution.py:25
  565.6 32.1 %collective-permute-start.17 = (bf16[3,1408,128]{1,2,0:T(8,128)(2,1)S(1)}, bf16[3,1408,128]{1,2,0:T(8,128)(2,1)S(1)}, u32[]{:S(2)}, u32[]{:S(2)}) collective-permute-start(bf16[3,1408,128]{1,2,0:T(8,128)(2,1)S(1)} %pad_maximum_fusion.7), channel_id=1, source_target_pairs={{0,16},{16,0},{1,17},{17,1},{2,18},{18,2},{3,19},{19,3},{4,20},{20... | collective-permute-start | bytes 3244040 | tf_op jit(solution)/shard_map/ppermute | solution.py:25
  602.6 11.2 %collective-permute-start.19 = (bf16[512,384]{1,0:T(8,128)(2,1)S(1)}, bf16[512,384]{1,0:T(8,128)(2,1)S(1)}, u32[]{:S(2)}, u32[]{:S(2)}) collective-permute-start(bf16[512,384]{1,0:T(8,128)(2,1)S(1)} %fusion.100), channel_id=1, source_target_pairs={{0,2},{1,3},{2,0},{3,1},{4,6},{5,7},{6,4},{7,5},{8,10},{9,11},{10,... | collective-permute-start | bytes 1179656 | tf_op jit(solution)/shard_map/ppermute | solution.py:30
  (48 other events, 710.1 us)
Sparse Core Ops, SparseCore 0:
  10.0 39.7 all-gather.18
  52.4 57.9 all-gather.20
  113.9 57.7 all-gather.22
  175.2 58.2 all-gather.24
  313.9 58.1 all-gather.26
  395.6 56.9 all-gather.28
  456.1 33.4 all-gather.30
  495.2 33.7 all-gather.32
